TPU v7x, 128 devices: a whole 4x4x4 slice. The times are simulated.
128 devices in a mesh: sp: 16 (over z, y), tp: 8 (over x, core).
Axes of the slice: x: 4, y: 4, z: 4, core: 2. Of those that a mesh axis runs over, the one named last changes fastest.
Arguments:
- tokens: bfloat16 [12288, 2048], P(('sp', 'tp')), may hold values from -6 to 6
- norm_gain: float32 [2048], replicated, may hold values from 0.1 to 1.9
- w_query: bfloat16 [2048, 1024], P('sp', 'tp'), may hold values from -0.125 to 0.125
- w_forget: bfloat16 [2048, 1024], P('sp', 'tp'), may hold values from -0.125 to 0.125
- w_input: bfloat16 [2048, 1024], P('sp', 'tp'), may hold values from -0.125 to 0.125
- w_outgate: bfloat16 [2048, 1024], P('sp', 'tp'), may hold values from -0.125 to 0.125
- w_conv_value: bfloat16 [2048, 1024], P('sp', 'tp'), may hold values from -0.125 to 0.125
- w_conv_gate: bfloat16 [2048, 1024], P('sp', 'tp'), may hold values from -0.125 to 0.125
- w_gate_rec: bfloat16 [2048, 2048], P('sp', 'tp'), may hold values from -0.125 to 0.125
- w_gate_conv: bfloat16 [2048, 2048], P('sp', 'tp'), may hold values from -0.125 to 0.125
- lower_bound: float32 [1024], P('tp'), may hold values from 0.92 to 0.9999593, as said below
- decay_shift: float32 [12288, 1024], P('sp', 'tp'), may hold values from -0.7 to 0, as said below
- state_init: float32 [8, 128, 128], P('tp'), may hold values from -0.125 to 0.125
- head_gain: float32 [1024], P('tp'), may hold values from 0.1 to 1.9
- conv_kernel: float32 [31, 1024], P(None, 'tp'), may hold values from -7.5 to 7.5
- channel_gain: float32 [1024], P('tp'), may hold values from 0.1 to 1.9
- channel_bias: float32 [1024], P('tp'), may hold values from -3 to 3
- w_out_rec: bfloat16 [1024, 2048], P('tp', 'sp'), may hold values from -0.1875 to 0.1875
- w_out_conv: bfloat16 [1024, 2048], P('tp', 'sp'), may hold values from -0.1875 to 0.1875
Outputs:
- mixed_out: bfloat16 [12288, 2048], P('sp', 'tp')
Inputs may be any that keep to these rules, and one draw needn't show every extreme that they name: `lower_bound`: every entry is below one. `decay_shift`: no entry is positive.
All inputs are finite; a program needn't handle non-finite values.
Results may differ from a plain program's by a relative error of at most 0.017.
Values may be sent and summed in bfloat16 or wider, within the bound.
A program may use at most 64 MiB of HBM per device.

v0:
```python
import jax
import jax.numpy as jnp
from jax import lax
from jax.sharding import PartitionSpec as P

HEAD = 128
CONV = 1024
KW = 31
BLOCK = 64
EPSILON = 1e-06


def in_one_piece(arrays, axis, dim, along):
    ends, at = ([], 0)
    for a in arrays[:-1]:
        at += a.shape[along]
        ends.append(at)
    both = jnp.concatenate(arrays, axis=along)
    return tuple(jnp.split(lax.all_gather(both, axis, axis=dim, tiled=True), ends, axis=along))


def sent_to_all(array, axis):
    size = lax.axis_size(axis)
    return lax.all_to_all(
        jnp.broadcast_to(array[None], (size, *array.shape)), axis, 0, 0, tiled=True
    )


def all_in_one(array, axis):
    leaves = jax.tree.leaves(array)
    sequence = sorted(range(len(leaves)), key=lambda k: -leaves[k].size)
    width = (1, *leaves[sequence[0]].shape)[-1]
    lines = [
        jnp.pad(leaves[k].reshape(-1), (0, -leaves[k].size % width)).reshape(-1, width)
        for k in sequence
    ]
    both, at, found = (sent_to_all(jnp.concatenate(lines), axis), 0, {})
    for k, line in zip(sequence, lines):
        section = both[:, at : at + len(line)].reshape(len(both), -1)
        found[k] = section[:, : leaves[k].size].reshape(-1, *leaves[k].shape)
        at += len(line)
    numbers = iter(range(len(leaves)))
    return jax.tree.map(lambda _: found[next(numbers)], array)


def joined_by_halves(pieces, combine):
    while len(jax.tree.leaves(pieces)[0]) > 1:
        pieces = jax.vmap(combine)(
            *(jax.tree.map(lambda part: part[side::2], pieces) for side in (0, 1))
        )
    return jax.tree.map(lambda part: part[0], pieces)


def entering(array, axis, combine, identity):
    size, position = (lax.axis_size(axis), lax.axis_index(axis))
    passed = jnp.arange(size) < position

    def kept(part, zero, own):
        part = jnp.where(
            passed.reshape(-1, *(1 for _ in own.shape)),
            part.astype(own.dtype),
            jnp.asarray(zero, own.dtype),
        )
        return part

    pieces = all_in_one(
        jax.tree.map(lambda part, kind: part.astype(kind), array, (jnp.bfloat16, jnp.bfloat16)),
        axis,
    )
    return joined_by_halves(jax.tree.map(kept, pieces, identity, array), combine)


def passed_along(block, axis, distance):
    devices = range(lax.axis_size(axis))
    route = [(i - distance, i) for i in devices if i - distance in devices]
    return lax.ppermute(block, axis, route)


def of_everyone(array, axis):
    everything = sent_to_all(array, axis)
    return jnp.sum(everything, axis=0)


def normalize_rows(values, gain_vector):
    widened = values.astype(jnp.float32)
    scale = lax.rsqrt(jnp.mean(widened * widened, axis=-1, keepdims=True) + EPSILON)
    return (widened * scale * gain_vector).astype(jnp.bfloat16)


def block_step(state, inputs):
    query, input_gate, values, log_decay = inputs
    length = query.shape[1]
    causal_masked = (jnp.arange(length)[:, None] >= jnp.arange(length)[None, :])[None, :, :, None]
    cumulative = jnp.cumsum(log_decay, axis=1)
    spread = cumulative[:, :, None, :] - cumulative[:, None, :, :]
    weight = jnp.where(causal_masked, jnp.exp(jnp.where(causal_masked, spread, 0.0)), 0.0)
    scores = jnp.einsum("htd,hsd,htsd->hts", query, input_gate, weight)
    output = jnp.einsum("hts,hsv->htv", scores, values)
    output = output + jnp.einsum("htd,hdv->htv", query * jnp.exp(cumulative), state)
    final = cumulative[:, -1:, :]
    carried = jnp.exp(final[:, 0, :])[:, :, None] * state
    carried = carried + jnp.einsum("hsd,hsv->hdv", input_gate * jnp.exp(final - cumulative), values)
    return (carried, output)


def compose(preceding_segment, later):
    return (preceding_segment[0] * later[0], later[0][..., None] * preceding_segment[1] + later[1])


def local(
    tokens,
    norm_gain,
    w_query,
    w_forget,
    w_input,
    w_outgate,
    w_conv_value,
    w_conv_gate,
    w_gate_rec,
    w_gate_conv,
    lower_bound,
    decay_shift,
    state_init,
    head_gain,
    conv_kernel,
    channel_gain,
    channel_bias,
    w_out_rec,
    w_out_conv,
):
    tp_count = lax.axis_size("tp")
    normed = normalize_rows(lax.all_gather(tokens, "tp", axis=0, tiled=True), norm_gain)
    row_count = normed.shape[0]
    weights = (
        w_query,
        w_forget,
        w_input,
        w_outgate,
        w_conv_value,
        w_conv_gate,
        w_gate_rec,
        w_gate_conv,
    )
    portions = in_one_piece(
        (
            weights[0],
            weights[1],
            weights[2],
            weights[3],
            weights[4],
            weights[5],
            weights[6],
            weights[7],
        ),
        "sp",
        0,
        1,
    )
    sums = tuple(
        (jnp.dot(normed, portion, preferred_element_type=jnp.float32) for portion in portions)
    )
    (
        query_raw,
        forget_raw,
        input_raw,
        outgate_raw,
        value_raw,
        gate_raw,
        gate_rec_raw,
        gate_conv_raw,
    ) = tuple((overall_aggregate.astype(jnp.bfloat16) for overall_aggregate in sums))
    local_heads = w_query.shape[1] // HEAD
    block_count = row_count // BLOCK
    query = jax.nn.silu(query_raw.astype(jnp.float32))
    input_gate = (1.0 - lower_bound) * jax.nn.sigmoid(-forget_raw.astype(jnp.float32))
    log_decay = jnp.log1p(-input_gate) + decay_shift
    values = input_raw.astype(jnp.float32)

    def to_blocks(array):
        return array.reshape(block_count, BLOCK, local_heads, HEAD).transpose(0, 2, 1, 3)

    zero_state = jnp.zeros((local_heads, HEAD, HEAD), jnp.float32)
    local_state, blocks_out = lax.scan(
        block_step,
        zero_state,
        (to_blocks(query), to_blocks(input_gate), to_blocks(values), to_blocks(log_decay)),
    )
    local_out = blocks_out.transpose(0, 2, 1, 3).reshape(row_count, local_heads, HEAD)
    running = jnp.cumsum(log_decay, axis=0)
    cumulated_forgetting = jnp.exp(running[-1]).reshape(local_heads, HEAD)
    ones_decay = jnp.ones_like(cumulated_forgetting)
    prefix_decay, prefix_state = entering(
        (cumulated_forgetting, local_state), "sp", compose, (ones_decay, zero_state)
    )
    incoming_state = prefix_decay[:, :, None] * state_init + prefix_state
    decayed_query = (query * jnp.exp(running)).reshape(row_count, local_heads, HEAD)
    head_out = local_out + jnp.einsum("thd,hdv->thv", decayed_query, incoming_state)
    head_out = head_out * lax.rsqrt(jnp.mean(head_out * head_out, axis=-1, keepdims=True) + EPSILON)
    head_out = head_out * head_gain.reshape(local_heads, HEAD)
    mixed_rec = (
        head_out.reshape(row_count, local_heads * HEAD)
        * jax.nn.silu(outgate_raw.astype(jnp.float32))
    ).astype(jnp.bfloat16)
    gated = (value_raw.astype(jnp.float32) * jax.nn.sigmoid(gate_raw.astype(jnp.float32))).astype(
        jnp.bfloat16
    )
    rim_width = KW - 1
    previous = passed_along(gated[row_count - rim_width :], "sp", 1)
    extended = jnp.concatenate([previous, gated], axis=0).astype(jnp.float32)
    conv_out = jnp.zeros((row_count, gated.shape[1]), jnp.float32)
    for tap_index in range(KW):
        conv_out = conv_out + conv_kernel[tap_index] * extended[tap_index : tap_index + row_count]
    squares = of_everyone(jnp.sum(conv_out * conv_out, axis=1), "tp")
    scale = lax.rsqrt(squares / CONV + EPSILON)[:, None]
    mixed_conv = jax.nn.silu(conv_out * scale * channel_gain + channel_bias).astype(jnp.bfloat16)
    rec_columns, conv_columns = in_one_piece((w_out_rec, w_out_conv), "sp", 1, 0)
    rec_width = mixed_rec.shape[1]
    rec_whole, conv_whole = in_one_piece((rec_columns, conv_columns), "tp", 0, 1)
    both = jnp.concatenate([mixed_rec, mixed_conv], axis=1).reshape(
        tp_count, row_count // tp_count, -1
    )
    arrived = lax.all_to_all(both, "tp", split_axis=0, concat_axis=2, tiled=True)
    item_count = arrived.shape[1]
    grouped = arrived.reshape(item_count, tp_count, -1)
    rec_part = grouped[:, :, :rec_width].reshape(item_count, -1)
    conv_part = grouped[:, :, rec_width:].reshape(item_count, -1)
    first = jnp.dot(rec_part, rec_whole, preferred_element_type=jnp.float32).astype(jnp.bfloat16)
    second = jnp.dot(conv_part, conv_whole, preferred_element_type=jnp.float32).astype(jnp.bfloat16)
    projected = jnp.stack([first, second], axis=1)[None]
    returned = lax.all_to_all(projected[0], "tp", split_axis=2, concat_axis=0, tiled=True)
    y_rec = returned[:, 0]
    y_conv = returned[:, 1]
    merged = jax.nn.sigmoid(gate_rec_raw.astype(jnp.float32)) * y_rec.astype(jnp.float32)
    merged = merged + jax.nn.sigmoid(gate_conv_raw.astype(jnp.float32)) * y_conv.astype(jnp.float32)
    return merged.astype(jnp.bfloat16)


def solution(mesh):
    in_specs = (
        P(("sp", "tp"), None),
        P(),
        P("sp", "tp"),
        P("sp", "tp"),
        P("sp", "tp"),
        P("sp", "tp"),
        P("sp", "tp"),
        P("sp", "tp"),
        P("sp", "tp"),
        P("sp", "tp"),
        P("tp"),
        P("sp", "tp"),
        P("tp", None, None),
        P("tp"),
        P(None, "tp"),
        P("tp"),
        P("tp"),
        P("tp", "sp"),
        P("tp", "sp"),
    )
    out_specs = P("sp", "tp")
    return jax.shard_map(local, mesh=mesh, in_specs=in_specs, out_specs=out_specs, check_vma=False)
```

profile of v0, /device:TPU:1, one launch (start us, length us, event | category | flops | bytes accessed | tf_op | source)
XLA Modules:
  0.0 333.0 jit_solution(5961914956780123622)
XLA Ops:
  19.8 34.6 %all-gather.9.cloned.1.call-done = bf16[256,2048]{1,0:T(8,128)(2,1)} async-done(((bf16[256,128]{1,0:T(8,128)(2,1)}), bf16[256,2048]{1,0:T(8,128)(2,1)}) %all-gather.9.cloned.1.call-update) | async-done | bytes 1048592 | tf_op jit(solution)/shard_map/all_gather | solution.py:19
  56.8 28.2 %all-gather.5.cloned.1.call-done = bf16[768,2048]{1,0:T(8,128)(2,1)} async-done(((bf16[96,2048]{1,0:T(8,128)(2,1)}), bf16[768,2048]{1,0:T(8,128)(2,1)}) %all-gather.5.cloned.1.call-update) | async-done | bytes 3145744 | tf_op jit(solution)/shard_map/all_gather | solution.py:132
  85.0 2.7 fusion.28
  88.6 54.3 %all-gather.7.cloned.1.call-done = bf16[2048,1280]{1,0:T(8,128)(2,1)} async-done(((bf16[128,1280]{1,0:T(8,128)(2,1)}), bf16[2048,1280]{1,0:T(8,128)(2,1)}) %all-gather.7.cloned.1.call-update) | async-done | bytes 5242896 | tf_op jit(solution)/shard_map/all_gather | solution.py:19
  142.9 2.8 divide_multiply_fusion
  145.7 2.1 convolution_convert_fusion.6
  147.7 2.9 log-plus-one_add_fusion
  150.7 80.2 %while.13 = (s32[]{:T(128)}, f32[1,128,128]{2,1,0:T(8,128)S(1)}, f32[12,1,64,128]{3,2,1,0:T(8,128)}, f32[12,1,64,128]{3,2,1,0:T(8,128)}, f32[12,1,64,128]{3,2,1,...) while((s32[]{:T(128)}, f32[1,128,128]{2,1,0:T(8,128)S(1)}, ...), condition=%wide.region_3.4_spmd.clone, body=%wide.region_1.3_spmd.clone.sunk | while | flops 9003011 | bytes 5051520 | solution.py:183
  153.0 1.7 fusion.167
  159.7 1.7 fusion.167
  166.3 1.7 fusion.167
  173.0 1.7 fusion.167
  179.7 1.7 fusion.167
  186.4 1.7 fusion.167
  193.1 1.7 fusion.167
  199.8 1.7 fusion.167
  206.4 1.7 fusion.167
  234.1 2.2 fusion.69
  236.5 2.0 fusion.68
  238.6 3.1 collective-permute-start
  245.3 5.5 %all-to-all-start.1 = ((f32[8,1,768]{2,1,0:T(1,128)}), f32[8,1,768]{2,1,0:T(1,128)}, u32[]{:S(2)}, u32[]{:S(2)}) async-start(f32[8,1,768]{2,1,0:T(1,128)} %broadcast_in_dim.89), calls=%async_computation.1 | async-start | bytes 49152 | tf_op jit(solution)/shard_map/all_to_all | solution.py:24
  252.2 3.4 %all-to-all-done.1 = f32[8,1,768]{2,1,0:T(1,128)} async-done(((f32[8,1,768]{2,1,0:T(1,128)}), f32[8,1,768]{2,1,0:T(1,128)}, u32[]{:S(2)}, u32[]{:S(2)}) %all-to-all-start.1) | async-done | bytes 24608 | tf_op jit(solution)/shard_map/all_to_all | solution.py:24
  257.3 7.0 %all-to-all-start = ((bf16[16,129,128]{2,1,0:T(8,128)(2,1)}), bf16[16,129,128]{2,1,0:T(8,128)(2,1)}, u32[]{:S(2)}, u32[]{:S(2)}) async-start(bf16[16,129,128]{2,1,0:T(8,128)(2,1)} %broadcast_in_dim.85), calls=%async_computation | async-start | bytes 1114112 | tf_op jit(solution)/shard_map/all_to_all | solution.py:24
  266.6 8.4 %all-to-all-done = bf16[16,129,128]{2,1,0:T(8,128)(2,1)} async-done(((bf16[16,129,128]{2,1,0:T(8,128)(2,1)}), bf16[16,129,128]{2,1,0:T(8,128)(2,1)}, u32[]{:S(2)}, u32[]{:S(2)}) %all-to-all-start) | async-done | bytes 528416 | tf_op jit(solution)/shard_map/all_to_all | solution.py:24
  278.2 2.1 fusion.117
  280.3 12.6 %all_to_all.44 = bf16[8,96,256]{2,1,0:T(8,128)(2,1)S(1)} all-to-all(bf16[8,96,256]{2,1,0:T(8,128)(2,1)S(1)} %bitcast.263), channel_id=1, replica_groups=mesh['sp'=16,'tp'=8] {'tp'}, dimensions={0} | all-to-all | bytes 786432 | tf_op jit(solution)/shard_map/all_to_all | solution.py:222
  293.0 3.0 fusion.44
  296.0 3.0 fusion.41
  299.8 18.2 %all_to_all.45 = bf16[96,2,2048]{0,1,2:T(2,128)(2,1)S(1)} all-to-all(bf16[96,2,2048]{0,1,2:T(2,128)(2,1)S(1)} %copy.78), channel_id=1, replica_groups=mesh['sp'=16,'tp'=8] {'tp'}, dimensions={2} | all-to-all | bytes 1572864 | tf_op jit(solution)/shard_map/all_to_all | solution.py:230
  318.1 1.9 copy.79
  320.0 3.4 %fusion.60 = f32[768,256]{1,0:T(8,128)S(1)} fusion(bf16[768,2048]{1,0:T(8,128)(2,1)} %copy-done.1, bf16[2048,1280]{1,0:T(8,128)(2,1)} %all-gather.7.cloned.1.call-done, bf16[768,2,256]{2,0,1:T(8,128)(2,1)} %bitcast.268), kind=kOutput, calls=%fused_computation.65 | convolution fusion | flops 806682624 | bytes 5373952 | tf_op jit(solution)/shard_map/dot_general | solution.py:160
  323.5 3.0 fusion.54
  (267 shorter events, 96.8 us)
Async XLA Ops:
  6.5 47.8 %all-gather.9.cloned.1.call-start = ((), (), s32[]{:S(2)}) async-start(), calls=%async_computation.6 | async-start | bytes 1114112 | tf_op jit(solution)/shard_map/all_gather | solution.py:19
  8.0 77.0 %all-gather.5.cloned.1.call-start = ((), (), s32[]{:S(2)}) async-start(), calls=%async_computation.4 | async-start | bytes 3538944 | tf_op jit(solution)/shard_map/all_gather | solution.py:132
  8.7 134.1 %all-gather.7.cloned.1.call-start = ((), (), s32[]{:S(2)}) async-start(), calls=%async_computation.5 | async-start | bytes 5570560 | tf_op jit(solution)/shard_map/all_gather | solution.py:19
  15.8 277.2 %all-gather.11.cloned.1.call-start = ((), (), s32[]{:S(2)}) async-start(), calls=%async_computation.7 | async-start | bytes 9437184 | tf_op jit(solution)/shard_map/all_gather | solution.py:19
  55.7 32.0 %copy-start.12 = (f32[2048]{0:T(1024)S(1)}, f32[2048]{0:T(1024)}, u32[]{:S(2)}) copy-start(f32[2048]{0:T(1024)} %param.22) | copy-start | bytes 24580
  88.6 189.6 %copy-start.1 = (bf16[768,2048]{1,0:T(8,128)(2,1)}, bf16[768,2048]{1,0:T(8,128)(2,1)S(1)}, u32[]{:S(2)}) copy-start(bf16[768,2048]{1,0:T(8,128)(2,1)S(1)} %fusion.30) | copy-start | bytes 9437188
  234.1 8.2 %copy-start.4 = (f32[128,6,128]{0,2,1:T(8,128)}, f32[128,6,128]{0,2,1:T(8,128)S(1)}, u32[]{:S(2)}) copy-start(f32[128,6,128]{0,2,1:T(8,128)S(1)} %copy.72) | copy-start | bytes 1179652
  236.3 6.6 %copy-start.13 = (f32[128]{0:T(128)S(1)}, f32[128]{0:T(128)}, u32[]{:S(2)}) copy-start(f32[128]{0:T(128)} %get-tuple-element.149) | copy-start | bytes 1540
  236.3 6.6 %copy-start.14 = (f32[128]{0:T(128)S(1)}, f32[128]{0:T(128)}, u32[]{:S(2)}) copy-start(f32[128]{0:T(128)} %get-tuple-element.150) | copy-start | bytes 1540
  236.3 6.6 %copy-start.15 = (f32[128]{0:T(128)S(1)}, f32[128]{0:T(128)}, u32[]{:S(2)}) copy-start(f32[128]{0:T(128)} %get-tuple-element.151) | copy-start | bytes 1540
  236.3 6.6 %copy-start.16 = (f32[128]{0:T(128)S(1)}, f32[128]{0:T(128)}, u32[]{:S(2)}) copy-start(f32[128]{0:T(128)} %get-tuple-element.152) | copy-start | bytes 1540
  236.3 6.6 %copy-start.17 = (f32[128]{0:T(128)S(1)}, f32[128]{0:T(128)}, u32[]{:S(2)}) copy-start(f32[128]{0:T(128)} %get-tuple-element.153) | copy-start | bytes 1540
  236.3 6.6 %copy-start.18 = (f32[128]{0:T(128)S(1)}, f32[128]{0:T(128)}, u32[]{:S(2)}) copy-start(f32[128]{0:T(128)} %get-tuple-element.154) | copy-start | bytes 1540
  236.3 6.6 %copy-start.19 = (f32[128]{0:T(128)S(1)}, f32[128]{0:T(128)}, u32[]{:S(2)}) copy-start(f32[128]{0:T(128)} %get-tuple-element.155) | copy-start | bytes 1540
  236.3 6.6 %copy-start.20 = (f32[128]{0:T(128)S(1)}, f32[128]{0:T(128)}, u32[]{:S(2)}) copy-start(f32[128]{0:T(128)} %get-tuple-element.156) | copy-start | bytes 1540
  236.4 6.6 %copy-start.21 = (f32[128]{0:T(128)S(1)}, f32[128]{0:T(128)}, u32[]{:S(2)}) copy-start(f32[128]{0:T(128)} %get-tuple-element.126) | copy-start | bytes 1540
  236.4 6.6 %copy-start.22 = (f32[128]{0:T(128)S(1)}, f32[128]{0:T(128)}, u32[]{:S(2)}) copy-start(f32[128]{0:T(128)} %get-tuple-element.127) | copy-start | bytes 1540
  236.4 6.6 %copy-start.23 = (f32[128]{0:T(128)S(1)}, f32[128]{0:T(128)}, u32[]{:S(2)}) copy-start(f32[128]{0:T(128)} %get-tuple-element.128) | copy-start | bytes 1540
  236.4 6.6 %copy-start.24 = (f32[128]{0:T(128)S(1)}, f32[128]{0:T(128)}, u32[]{:S(2)}) copy-start(f32[128]{0:T(128)} %get-tuple-element.129) | copy-start | bytes 1540
  236.4 6.6 %copy-start.25 = (f32[128]{0:T(128)S(1)}, f32[128]{0:T(128)}, u32[]{:S(2)}) copy-start(f32[128]{0:T(128)} %get-tuple-element.130) | copy-start | bytes 1540
  236.4 6.6 %copy-start.26 = (f32[128]{0:T(128)S(1)}, f32[128]{0:T(128)}, u32[]{:S(2)}) copy-start(f32[128]{0:T(128)} %get-tuple-element.131) | copy-start | bytes 1540
  236.4 6.6 %copy-start.27 = (f32[128]{0:T(128)S(1)}, f32[128]{0:T(128)}, u32[]{:S(2)}) copy-start(f32[128]{0:T(128)} %get-tuple-element.132) | copy-start | bytes 1540
  236.4 6.6 %copy-start.28 = (f32[128]{0:T(128)S(1)}, f32[128]{0:T(128)}, u32[]{:S(2)}) copy-start(f32[128]{0:T(128)} %get-tuple-element.133) | copy-start | bytes 1540
  236.4 6.6 %copy-start.29 = (f32[128]{0:T(128)S(1)}, f32[128]{0:T(128)}, u32[]{:S(2)}) copy-start(f32[128]{0:T(128)} %get-tuple-element.134) | copy-start | bytes 1540
  236.4 6.6 %copy-start.30 = (f32[128]{0:T(128)S(1)}, f32[128]{0:T(128)}, u32[]{:S(2)}) copy-start(f32[128]{0:T(128)} %get-tuple-element.135) | copy-start | bytes 1540
  236.5 6.6 %copy-start.31 = (f32[128]{0:T(128)S(1)}, f32[128]{0:T(128)}, u32[]{:S(2)}) copy-start(f32[128]{0:T(128)} %get-tuple-element.136) | copy-start | bytes 1540
  236.5 6.6 %copy-start.32 = (f32[128]{0:T(128)S(1)}, f32[128]{0:T(128)}, u32[]{:S(2)}) copy-start(f32[128]{0:T(128)} %get-tuple-element.137) | copy-start | bytes 1540
  238.6 4.3 %collective-permute-start = (bf16[30,128]{1,0:T(8,128)(2,1)S(1)}, bf16[30,128]{1,0:T(8,128)(2,1)S(1)}, u32[]{:S(2)}, u32[]{:S(2)}) collective-permute-start(bf16[30,128]{1,0:T(8,128)(2,1)S(1)} %slice.369), channel_id=1, source_target_pairs={{0,8},{8,16},{16,24},{24,32},{32,40},{40,48},{48,56},{56,64},{64,7... | collective-permute-start | bytes 23048 | tf_op jit(solution)/shard_map/ppermute | solution.py:76
  245.3 10.3 %all-to-all-start.1 = ((f32[8,1,768]{2,1,0:T(1,128)}), f32[8,1,768]{2,1,0:T(1,128)}, u32[]{:S(2)}, u32[]{:S(2)}) async-start(f32[8,1,768]{2,1,0:T(1,128)} %broadcast_in_dim.89), calls=%async_computation.1 | async-start | bytes 49152 | tf_op jit(solution)/shard_map/all_to_all | solution.py:24
  257.3 17.8 %all-to-all-start = ((bf16[16,129,128]{2,1,0:T(8,128)(2,1)}), bf16[16,129,128]{2,1,0:T(8,128)(2,1)}, u32[]{:S(2)}, u32[]{:S(2)}) async-start(bf16[16,129,128]{2,1,0:T(8,128)(2,1)} %broadcast_in_dim.85), calls=%async_computation | async-start | bytes 1114112 | tf_op jit(solution)/shard_map/all_to_all | solution.py:24
  266.6 11.1 %copy-start.5 = (f32[128,6,128]{0,2,1:T(8,128)S(1)}, f32[128,6,128]{0,2,1:T(8,128)}, u32[]{:S(2)}) copy-start(f32[128,6,128]{0,2,1:T(8,128)} %copy-done.4) | copy-start | bytes 1179652
  266.6 11.5 %copy-start.41 = (f32[128]{0:T(128)S(1)}, f32[128]{0:T(128)}, u32[]{:S(2)}) copy-start(f32[128]{0:T(128)} %param.34) | copy-start | bytes 1540
  (17 other events, 69.8 us)
Sparse Core Ops, SparseCore 0:
  9.4 44.8 all-gather.8
  56.0 28.8 all-gather.4
  87.1 55.7 all-gather.6
  144.4 49.7 all-gather.10
where the time goes:
time: 338 us; the launch traced here: 333 us
  waiting for transfers between devices  130 us (38%)
  matrix products  58.7 us (17%)
  other arithmetic  47.2 us (14%)
  local copies, waits for them, and re-layouts  36.5 us (11%)
  blocking collectives  30.8 us (9%)
  starting transfers between devices  15.8 us (5%)
  between operations  13.9 us (4%)
    all_gather x3, waiting for transfers between devices, in_one_piece(): lax.all_gather(both, axis, axis=dim, tiled=True)  88.9 us
    all_gather x1, waiting for transfers between devices, local(): lax.all_gather(tokens, 'tp', axis=0, tiled=True)  28.2 us
    dot_general x12, other arithmetic, block_step(): scores = jnp.einsum('htd,hsd,htsd->hts', query, input_gate, weight)  20.5 us
    dot_general x8, matrix products, local(): jnp.dot(normed, portion, preferred_element_type=jnp.float32)  20.5 us
    all_to_all x1, blocking collectives, local(): lax.all_to_all(projected[0], 'tp', split_axis=2, concat_axis=0, tiled=True)  18.2 us
    dot_general x12, matrix products, block_step(): jnp.einsum('htd,hdv->htv', query * jnp.exp(cumulative), state)  18.2 us
    all_to_all x2, starting transfers between devices, sent_to_all(): lax.all_to_all(jnp.broadcast_to(array[None], (size, *array.shape)), axis,...  12.6 us
    all_to_all x1, blocking collectives, local(): lax.all_to_all(both, 'tp', split_axis=0, concat_axis=2, tiled=True)  12.6 us
  transfers between devices with their start and end apart: 7, of which 5 were waited for; matrix products, arithmetic and copies ran while one was open for 37% of the time, Pallas kernels for 0%

commit v1 on v0

--- a/solution.py
+++ b/solution.py
@@ -8,6 +8,11 @@
 KW = 31
 BLOCK = 64
 EPSILON = 1e-06
+
+
+def tiled_gather(shard, axis, dim):
+    copies = jnp.concatenate([shard] * lax.axis_size(axis), axis=dim)
+    return lax.all_to_all(copies, axis, dim, dim, tiled=True)
 
 
 def in_one_piece(arrays, axis, dim, along):
@@ -129,7 +134,7 @@
     w_out_conv,
 ):
     tp_count = lax.axis_size("tp")
-    normed = normalize_rows(lax.all_gather(tokens, "tp", axis=0, tiled=True), norm_gain)
+    normed = normalize_rows(tiled_gather(tokens, "tp", 0), norm_gain)
     row_count = normed.shape[0]
     weights = (
         w_query,

time: 338 us -> 310 us (0.917)
  waiting for transfers between devices: 130 us -> 92.6 us
  starting transfers between devices: 15.8 us -> 21.6 us
    all_gather x1 -> x0, waiting for transfers between devices: 28.2 us -> none  [local(): lax.all_gather(tokens, 'tp', axis=0, tiled=True)]
    all_gather x3, waiting for transfers between devices: 88.9 us -> 74.2 us  [in_one_piece(): lax.all_gather(both, axis, axis=dim, tiled=True)]
    all_to_all x0 -> x1, waiting for transfers between devices: none -> 6.52 us  [tiled_gather(): return lax.all_to_all(copies, axis, dim, dim, tiled=True)]
    all_to_all x0 -> x1, starting transfers between devices: none -> 5.92 us  [tiled_gather(): return lax.all_to_all(copies, axis, dim, dim, tiled=True)]
    unnamed x92 -> x105, local copies, waits for them, and re-layouts: 7.34 us -> 12 us
  transfers between devices with their start and end apart: 7 -> 7, of which waited for: 5 -> 5; matrix products, arithmetic and copies ran while one was open for 37% -> 41% of each run, Pallas kernels for 0% -> 0%
where the time goes in v1:
time: 310 us; the launch traced here: 305 us
  waiting for transfers between devices  92.6 us (30%)
  matrix products  59.7 us (19%)
  other arithmetic  46.2 us (15%)
  local copies, waits for them, and re-layouts  39.4 us (13%)
  blocking collectives  30.8 us (10%)
  starting transfers between devices  21.6 us (7%)
  between operations  13.9 us (4%)
    all_gather x3, waiting for transfers between devices, in_one_piece(): lax.all_gather(both, axis, axis=dim, tiled=True)  74.2 us
    dot_general x8, matrix products, local(): jnp.dot(normed, portion, preferred_element_type=jnp.float32)  21.4 us
    dot_general x12, other arithmetic, block_step(): scores = jnp.einsum('htd,hsd,htsd->hts', query, input_gate, weight)  20.5 us
    all_to_all x1, blocking collectives, local(): lax.all_to_all(projected[0], 'tp', split_axis=2, concat_axis=0, tiled=True)  18.2 us
    dot_general x12, matrix products, block_step(): jnp.einsum('htd,hdv->htv', query * jnp.exp(cumulative), state)  18.2 us
    all_to_all x2, starting transfers between devices, sent_to_all(): lax.all_to_all(jnp.broadcast_to(array[None], (size, *array.shape)), axis,...  12.6 us
    all_to_all x1, blocking collectives, local(): lax.all_to_all(both, 'tp', split_axis=0, concat_axis=2, tiled=True)  12.5 us
    unnamed x105, local copies, waits for them, and re-layouts  12 us
  transfers between devices with their start and end apart: 7, of which 5 were waited for; matrix products, arithmetic and copies ran while one was open for 41% of the time, Pallas kernels for 0%

profile of v1, /device:TPU:1, one launch (start us, length us, event | category | flops | bytes accessed | tf_op | source)
XLA Modules:
  0.0 304.6 jit_solution(1731135993575298035)
XLA Ops:
  20.0 5.9 %all-to-all-start = ((bf16[8,96,2048]{2,1,0:T(8,128)(2,1)}), bf16[8,96,2048]{2,1,0:T(8,128)(2,1)S(1)}, u32[]{:S(2)}, u32[]{:S(2)}) async-start(bf16[8,96,2048]{2,1,0:T(8,128)(2,1)} %bitcast.267), calls=%async_computation | async-start | bytes 6291456 | tf_op jit(solution)/shard_map/all_to_all | solution.py:15
  27.2 27.2 %all-gather.6.cloned.1.call-done = bf16[256,2048]{1,0:T(8,128)(2,1)} async-done(((bf16[256,128]{1,0:T(8,128)(2,1)}), bf16[256,2048]{1,0:T(8,128)(2,1)}) %all-gather.6.cloned.1.call-update) | async-done | bytes 1048592 | tf_op jit(solution)/shard_map/all_gather | solution.py:24
  56.9 6.5 %all-to-all-done = bf16[8,96,2048]{2,1,0:T(8,128)(2,1)S(1)} async-done(((bf16[8,96,2048]{2,1,0:T(8,128)(2,1)}), bf16[8,96,2048]{2,1,0:T(8,128)(2,1)S(1)}, u32[]{:S(2)}, u32[]{:S(2)}) %all-to-all-start) | async-done | bytes 3145760 | tf_op jit(solution)/shard_map/all_to_all | solution.py:15
  64.2 2.4 fusion.29
  66.6 47.0 %all-gather.4.cloned.1.call-done = bf16[2048,1280]{1,0:T(8,128)(2,1)} async-done(((bf16[128,1280]{1,0:T(8,128)(2,1)}), bf16[2048,1280]{1,0:T(8,128)(2,1)}) %all-gather.4.cloned.1.call-update) | async-done | bytes 5242896 | tf_op jit(solution)/shard_map/all_gather | solution.py:24
  113.5 3.7 %divide_multiply_fusion = f32[768,128]{1,0:T(8,128)} fusion(bf16[768,2048]{1,0:T(8,128)(2,1)} %fusion.29, bf16[2048,1280]{1,0:T(8,128)(2,1)} %all-gather.4.cloned.1.call-done), kind=kOutput, calls=%fused_computation.173 | convolution fusion | flops 403243008 | bytes 4063232 | tf_op jit(solution)/shard_map/dot_general | solution.py:165
  117.3 2.1 convolution_convert_fusion.6
  119.4 2.9 log-plus-one_add_fusion
  122.3 80.2 %while.13 = (s32[]{:T(128)}, f32[1,128,128]{2,1,0:T(8,128)S(1)}, f32[12,1,64,128]{3,2,1,0:T(8,128)}, f32[12,1,64,128]{3,2,1,0:T(8,128)}, f32[12,1,64,128]{3,2,1,...) while((s32[]{:T(128)}, f32[1,128,128]{2,1,0:T(8,128)S(1)}, ...), condition=%wide.region_3.4_spmd.clone, body=%wide.region_1.3_spmd.clone.sunk | while | flops 9003011 | bytes 5051520 | solution.py:188
  124.6 1.7 fusion.166
  131.3 1.7 fusion.166
  138.0 1.7 fusion.166
  144.7 1.7 fusion.166
  151.3 1.7 fusion.166
  158.0 1.7 fusion.166
  164.7 1.7 fusion.166
  198.1 1.7 fusion.166
  205.7 2.2 fusion.68
  208.2 2.0 fusion.67
  210.2 3.1 %collective-permute-start = (bf16[30,128]{1,0:T(8,128)(2,1)S(1)}, bf16[30,128]{1,0:T(8,128)(2,1)S(1)}, u32[]{:S(2)}, u32[]{:S(2)}) collective-permute-start(bf16[30,128]{1,0:T(8,128)(2,1)S(1)} %slice.369), channel_id=1, source_target_pairs={{0,8},{8,16},{16,24},{24,32},{32,40},{40,48},{48,56},{56,64},{64,7... | collective-permute-start | bytes 23048 | tf_op jit(solution)/shard_map/ppermute | solution.py:81
  216.9 5.6 %all-to-all-start.2 = ((f32[8,1,768]{2,1,0:T(1,128)}), f32[8,1,768]{2,1,0:T(1,128)}, u32[]{:S(2)}, u32[]{:S(2)}) async-start(f32[8,1,768]{2,1,0:T(1,128)} %broadcast_in_dim.89), calls=%async_computation.2 | async-start | bytes 49152 | tf_op jit(solution)/shard_map/all_to_all | solution.py:29
  223.8 3.4 %all-to-all-done.2 = f32[8,1,768]{2,1,0:T(1,128)} async-done(((f32[8,1,768]{2,1,0:T(1,128)}), f32[8,1,768]{2,1,0:T(1,128)}, u32[]{:S(2)}, u32[]{:S(2)}) %all-to-all-start.2) | async-done | bytes 24608 | tf_op jit(solution)/shard_map/all_to_all | solution.py:29
  228.9 7.0 %all-to-all-start.1 = ((bf16[16,129,128]{2,1,0:T(8,128)(2,1)}), bf16[16,129,128]{2,1,0:T(8,128)(2,1)}, u32[]{:S(2)}, u32[]{:S(2)}) async-start(bf16[16,129,128]{2,1,0:T(8,128)(2,1)} %broadcast_in_dim.85), calls=%async_computation.1 | async-start | bytes 1114112 | tf_op jit(solution)/shard_map/all_to_all | solution.py:29
  238.3 8.4 %all-to-all-done.1 = bf16[16,129,128]{2,1,0:T(8,128)(2,1)} async-done(((bf16[16,129,128]{2,1,0:T(8,128)(2,1)}), bf16[16,129,128]{2,1,0:T(8,128)(2,1)}, u32[]{:S(2)}, u32[]{:S(2)}) %all-to-all-start.1) | async-done | bytes 528416 | tf_op jit(solution)/shard_map/all_to_all | solution.py:29
  249.8 2.1 fusion.116
  252.0 12.5 %all_to_all.53 = bf16[8,96,256]{2,1,0:T(8,128)(2,1)S(1)} all-to-all(bf16[8,96,256]{2,1,0:T(8,128)(2,1)S(1)} %bitcast.271), channel_id=1, replica_groups=mesh['sp'=16,'tp'=8] {'tp'}, dimensions={0} | all-to-all | bytes 786432 | tf_op jit(solution)/shard_map/all_to_all | solution.py:227
  264.6 3.0 fusion.43
  267.6 3.0 fusion.40
  271.5 18.2 %all_to_all.54 = bf16[96,2,2048]{0,1,2:T(2,128)(2,1)S(1)} all-to-all(bf16[96,2,2048]{0,1,2:T(2,128)(2,1)S(1)} %copy.78), channel_id=1, replica_groups=mesh['sp'=16,'tp'=8] {'tp'}, dimensions={2} | all-to-all | bytes 1572864 | tf_op jit(solution)/shard_map/all_to_all | solution.py:235
  289.7 1.9 copy.79
  291.6 3.4 %fusion.59 = f32[768,256]{1,0:T(8,128)S(1)} fusion(bf16[768,2048]{1,0:T(8,128)(2,1)} %fusion.29, bf16[2048,1280]{1,0:T(8,128)(2,1)} %all-gather.4.cloned.1.call-done, bf16[768,2,256]{2,0,1:T(8,128)(2,1)} %bitcast.276), kind=kOutput, calls=%fused_computation.64 | convolution fusion | flops 806682624 | bytes 5373952 | tf_op jit(solution)/shard_map/dot_general | solution.py:165
  295.1 3.0 fusion.53
  (281 shorter events, 99.9 us)
Async XLA Ops:
  6.5 11.7 %copy-start = (bf16[96,2048]{1,0:T(8,128)(2,1)S(1)}, bf16[96,2048]{1,0:T(8,128)(2,1)}, u32[]{:S(2)}) copy-start(bf16[96,2048]{1,0:T(8,128)(2,1)} %param.21) | copy-start | bytes 1179652
  6.5 47.9 %all-gather.6.cloned.1.call-start = ((), (), s32[]{:S(2)}) async-start(), calls=%async_computation.6 | async-start | bytes 1114112 | tf_op jit(solution)/shard_map/all_gather | solution.py:24
  8.0 105.5 %all-gather.4.cloned.1.call-start = ((), (), s32[]{:S(2)}) async-start(), calls=%async_computation.5 | async-start | bytes 5570560 | tf_op jit(solution)/shard_map/all_gather | solution.py:24
  20.0 43.4 %all-to-all-start = ((bf16[8,96,2048]{2,1,0:T(8,128)(2,1)}), bf16[8,96,2048]{2,1,0:T(8,128)(2,1)S(1)}, u32[]{:S(2)}, u32[]{:S(2)}) async-start(bf16[8,96,2048]{2,1,0:T(8,128)(2,1)} %bitcast.267), calls=%async_computation | async-start | bytes 6291456 | tf_op jit(solution)/shard_map/all_to_all | solution.py:15
  25.9 238.7 %all-gather.8.cloned.1.call-start = ((), (), s32[]{:S(2)}) async-start(), calls=%async_computation.7 | async-start | bytes 9437184 | tf_op jit(solution)/shard_map/all_gather | solution.py:24
  55.7 8.4 %copy-start.14 = (f32[2048]{0:T(1024)S(1)}, f32[2048]{0:T(1024)}, u32[]{:S(2)}) copy-start(f32[2048]{0:T(1024)} %param.22) | copy-start | bytes 24580
  66.6 50.7 %copy-start.2 = (bf16[768,2048]{1,0:T(8,128)(2,1)S(1)}, bf16[768,2048]{1,0:T(8,128)(2,1)}, u32[]{:S(2)}) copy-start(bf16[768,2048]{1,0:T(8,128)(2,1)} %fusion.29) | copy-start | bytes 9437188
  205.7 8.2 %copy-start.5 = (f32[128,6,128]{0,2,1:T(8,128)}, f32[128,6,128]{0,2,1:T(8,128)S(1)}, u32[]{:S(2)}) copy-start(f32[128,6,128]{0,2,1:T(8,128)S(1)} %copy.72) | copy-start | bytes 1179652
  207.9 6.6 %copy-start.15 = (f32[128]{0:T(128)S(1)}, f32[128]{0:T(128)}, u32[]{:S(2)}) copy-start(f32[128]{0:T(128)} %get-tuple-element.149) | copy-start | bytes 1540
  207.9 6.6 %copy-start.16 = (f32[128]{0:T(128)S(1)}, f32[128]{0:T(128)}, u32[]{:S(2)}) copy-start(f32[128]{0:T(128)} %get-tuple-element.150) | copy-start | bytes 1540
  207.9 6.6 %copy-start.17 = (f32[128]{0:T(128)S(1)}, f32[128]{0:T(128)}, u32[]{:S(2)}) copy-start(f32[128]{0:T(128)} %get-tuple-element.151) | copy-start | bytes 1540
  207.9 6.6 %copy-start.18 = (f32[128]{0:T(128)S(1)}, f32[128]{0:T(128)}, u32[]{:S(2)}) copy-start(f32[128]{0:T(128)} %get-tuple-element.152) | copy-start | bytes 1540
  207.9 6.6 %copy-start.19 = (f32[128]{0:T(128)S(1)}, f32[128]{0:T(128)}, u32[]{:S(2)}) copy-start(f32[128]{0:T(128)} %get-tuple-element.153) | copy-start | bytes 1540
  207.9 6.6 %copy-start.20 = (f32[128]{0:T(128)S(1)}, f32[128]{0:T(128)}, u32[]{:S(2)}) copy-start(f32[128]{0:T(128)} %get-tuple-element.154) | copy-start | bytes 1540
  207.9 6.6 %copy-start.21 = (f32[128]{0:T(128)S(1)}, f32[128]{0:T(128)}, u32[]{:S(2)}) copy-start(f32[128]{0:T(128)} %get-tuple-element.155) | copy-start | bytes 1540
  208.0 6.6 %copy-start.22 = (f32[128]{0:T(128)S(1)}, f32[128]{0:T(128)}, u32[]{:S(2)}) copy-start(f32[128]{0:T(128)} %get-tuple-element.156) | copy-start | bytes 1540
  208.0 6.6 %copy-start.23 = (f32[128]{0:T(128)S(1)}, f32[128]{0:T(128)}, u32[]{:S(2)}) copy-start(f32[128]{0:T(128)} %get-tuple-element.126) | copy-start | bytes 1540
  208.0 6.6 %copy-start.24 = (f32[128]{0:T(128)S(1)}, f32[128]{0:T(128)}, u32[]{:S(2)}) copy-start(f32[128]{0:T(128)} %get-tuple-element.127) | copy-start | bytes 1540
  208.0 6.6 %copy-start.25 = (f32[128]{0:T(128)S(1)}, f32[128]{0:T(128)}, u32[]{:S(2)}) copy-start(f32[128]{0:T(128)} %get-tuple-element.128) | copy-start | bytes 1540
  208.0 6.6 %copy-start.26 = (f32[128]{0:T(128)S(1)}, f32[128]{0:T(128)}, u32[]{:S(2)}) copy-start(f32[128]{0:T(128)} %get-tuple-element.129) | copy-start | bytes 1540
  208.0 6.6 %copy-start.27 = (f32[128]{0:T(128)S(1)}, f32[128]{0:T(128)}, u32[]{:S(2)}) copy-start(f32[128]{0:T(128)} %get-tuple-element.130) | copy-start | bytes 1540
  208.0 6.6 %copy-start.28 = (f32[128]{0:T(128)S(1)}, f32[128]{0:T(128)}, u32[]{:S(2)}) copy-start(f32[128]{0:T(128)} %get-tuple-element.131) | copy-start | bytes 1540
  208.0 6.6 %copy-start.29 = (f32[128]{0:T(128)S(1)}, f32[128]{0:T(128)}, u32[]{:S(2)}) copy-start(f32[128]{0:T(128)} %get-tuple-element.132) | copy-start | bytes 1540
  208.0 6.6 %copy-start.30 = (f32[128]{0:T(128)S(1)}, f32[128]{0:T(128)}, u32[]{:S(2)}) copy-start(f32[128]{0:T(128)} %get-tuple-element.133) | copy-start | bytes 1540
  208.1 6.6 %copy-start.31 = (f32[128]{0:T(128)S(1)}, f32[128]{0:T(128)}, u32[]{:S(2)}) copy-start(f32[128]{0:T(128)} %get-tuple-element.134) | copy-start | bytes 1540
  208.1 6.6 %copy-start.32 = (f32[128]{0:T(128)S(1)}, f32[128]{0:T(128)}, u32[]{:S(2)}) copy-start(f32[128]{0:T(128)} %get-tuple-element.135) | copy-start | bytes 1540
  208.1 6.6 %copy-start.33 = (f32[128]{0:T(128)S(1)}, f32[128]{0:T(128)}, u32[]{:S(2)}) copy-start(f32[128]{0:T(128)} %get-tuple-element.136) | copy-start | bytes 1540
  210.2 4.3 %collective-permute-start = (bf16[30,128]{1,0:T(8,128)(2,1)S(1)}, bf16[30,128]{1,0:T(8,128)(2,1)S(1)}, u32[]{:S(2)}, u32[]{:S(2)}) collective-permute-start(bf16[30,128]{1,0:T(8,128)(2,1)S(1)} %slice.369), channel_id=1, source_target_pairs={{0,8},{8,16},{16,24},{24,32},{32,40},{40,48},{48,56},{56,64},{64,7... | collective-permute-start | bytes 23048 | tf_op jit(solution)/shard_map/ppermute | solution.py:81
  216.9 10.4 %all-to-all-start.2 = ((f32[8,1,768]{2,1,0:T(1,128)}), f32[8,1,768]{2,1,0:T(1,128)}, u32[]{:S(2)}, u32[]{:S(2)}) async-start(f32[8,1,768]{2,1,0:T(1,128)} %broadcast_in_dim.89), calls=%async_computation.2 | async-start | bytes 49152 | tf_op jit(solution)/shard_map/all_to_all | solution.py:29
  228.9 17.8 %all-to-all-start.1 = ((bf16[16,129,128]{2,1,0:T(8,128)(2,1)}), bf16[16,129,128]{2,1,0:T(8,128)(2,1)}, u32[]{:S(2)}, u32[]{:S(2)}) async-start(bf16[16,129,128]{2,1,0:T(8,128)(2,1)} %broadcast_in_dim.85), calls=%async_computation.1 | async-start | bytes 1114112 | tf_op jit(solution)/shard_map/all_to_all | solution.py:29
  238.3 11.1 %copy-start.6 = (f32[128,6,128]{0,2,1:T(8,128)S(1)}, f32[128,6,128]{0,2,1:T(8,128)}, u32[]{:S(2)}) copy-start(f32[128,6,128]{0,2,1:T(8,128)} %copy-done.5) | copy-start | bytes 1179652
  238.3 11.5 %copy-start.44 = (f32[128]{0:T(128)S(1)}, f32[128]{0:T(128)}, u32[]{:S(2)}) copy-start(f32[128]{0:T(128)} %param.34) | copy-start | bytes 1540
  (20 other events, 87.1 us)
Sparse Core Ops, SparseCore 0:
  9.4 44.9 all-gather.5
  56.6 56.9 all-gather.3
  115.3 49.7 all-gather.7
